TPU v7x, 32 devices: a whole 2x2x4 slice. The times are simulated.
32 devices in a mesh: grp: 1, ep: 4 (over z), tp: 8 (over y, x, core).
Axes of the slice: x: 2, y: 2, z: 4, core: 2. Of those that a mesh axis runs over, the one named last changes fastest.
Arguments:
- tokens: bfloat16 [256, 2048], P(('grp', 'ep')), may hold values from -6 to 6
- norm_gain: float32 [2048], replicated, may hold values from 0.1 to 1.9
- routes: int32 [256, 8], P(('grp', 'ep')), may hold values from 0 to 15, all different within a row; in each aligned block of 64 rows (0 to 63, 64 to 127, ...) at most 64 rows name the same one
- route_weight: float32 [256, 8], P(('grp', 'ep')), may hold values from 0.05 to 1
- gate_proj: bfloat16 [32, 2048, 256], P(('ep', 'tp')), may hold values from -0.125 to 0.125
- up_proj: bfloat16 [32, 2048, 256], P(('ep', 'tp')), may hold values from -0.125 to 0.125
- down_proj: bfloat16 [32, 256, 2048], P(('ep', 'tp')), may hold values from -0.25 to 0.25
- shared_gate: bfloat16 [2048, 512], P(None, 'tp'), may hold values from -0.125 to 0.125
- shared_up: bfloat16 [2048, 512], P(None, 'tp'), may hold values from -0.125 to 0.125
- shared_down: bfloat16 [512, 2048], P('tp'), may hold values from -0.25 to 0.25
Outputs:
- mixed: bfloat16 [256, 2048], P(('grp', 'ep'), 'tp')
Inputs may be any that keep to these rules, and one draw needn't show every extreme that they name: `routes`: each row names 8 different experts. Among the 64 rows of one ep index no expert is named by more than 64 rows, a bound that some block reaches of them.
All inputs are finite; a program needn't handle non-finite values.
Results may differ from a plain program's by a relative error of at most 0.0064.
Values may be sent and summed in bfloat16 or wider, within the bound.
A program may use at most 64 MiB of HBM per device.

v0:
```python
import jax
import jax.numpy as jnp
from jax import lax
from jax.sharding import PartitionSpec as P

EXPERT_SHARDS = 2


eps = 1e-06
routed_scale = 2.5


def norm_rows(tokens, norm_gain):
    values = tokens.astype(jnp.float32)
    scaled = values * lax.rsqrt(jnp.mean(values * values, axis=-1, keepdims=True) + eps)
    return (scaled * norm_gain).astype(jnp.bfloat16)


def expert_apply(row_block, gate_half, up_half, down_half):
    gate_part = jnp.dot(row_block, gate_half, preferred_element_type=jnp.float32)
    upper = jnp.dot(row_block, up_half, preferred_element_type=jnp.float32)
    active = (jax.nn.silu(gate_part) * upper).astype(jnp.bfloat16)
    return jnp.dot(active, down_half, preferred_element_type=jnp.float32)


def slot_table(hit_table, capacity):
    counts = jnp.cumsum(hit_table.astype(jnp.int32), axis=1) - 1
    slots = jnp.arange(capacity, dtype=jnp.int32)
    return hit_table[:, None, :] & (counts[:, None, :] == slots[None, :, None])


def per_device(
    tokens,
    norm_gain,
    routes,
    route_weight,
    gate_proj,
    up_proj,
    down_proj,
    shared_gate,
    shared_up,
    shared_down,
):
    ep_count = lax.axis_size("ep")
    tp_count = lax.axis_size("tp")
    per_block = tp_count // EXPERT_SHARDS
    experts = ep_count * per_block
    tok_rows, top_count = routes.shape
    capacity = min(tok_rows, max(2, 2 * tok_rows * top_count // experts))
    column = lax.axis_index("tp") // EXPERT_SHARDS
    normed = norm_rows(tokens, norm_gain)
    mixing = route_weight / jnp.sum(route_weight, axis=1, keepdims=True) * routed_scale
    targets = jnp.arange(ep_count, dtype=jnp.int32) * per_block + column
    matches = routes[:, :, None] == targets[None, None, :]
    sent_hits = jnp.any(matches, axis=1).T
    weights_out = jnp.sum(jnp.where(matches, mixing[:, :, None], 0.0), axis=1).T
    sending = slot_table(sent_hits, capacity)
    gate_half = gate_proj[0]
    up_half = up_proj[0]
    down_half = down_proj[0]
    outgoing = jnp.einsum(
        "kct,td->kcd", sending.astype(jnp.bfloat16), normed, preferred_element_type=jnp.float32
    ).astype(jnp.bfloat16)
    arrived = lax.all_to_all(outgoing, "ep", split_axis=0, concat_axis=0, tiled=True)
    sources, slot_count, feature_width = arrived.shape
    produced = expert_apply(
        arrived.reshape(sources * slot_count, feature_width), gate_half, up_half, down_half
    )
    produced = produced.reshape(sources, slot_count, -1)
    returned = lax.all_to_all(produced, "ep", split_axis=0, concat_axis=0, tiled=True)
    weighting = sending.astype(jnp.float32) * weights_out[:, None, :]
    routed = jnp.einsum("kct,kcd->td", weighting, returned, precision=lax.Precision.HIGHEST)
    shared_term = expert_apply(normed, shared_gate, shared_up, shared_down)
    return lax.psum_scatter(routed + shared_term, "tp", scatter_dimension=1, tiled=True).astype(
        jnp.bfloat16
    )


def solution(mesh):
    in_specs = (
        P(("grp", "ep"), None),
        P(),
        P(("grp", "ep"), None),
        P(("grp", "ep"), None),
        P(("ep", "tp"), None, None),
        P(("ep", "tp"), None, None),
        P(("ep", "tp"), None, None),
        P(None, "tp"),
        P(None, "tp"),
        P("tp", None),
    )
    out_specs = P(("grp", "ep"), "tp")
    return jax.shard_map(
        per_device, mesh=mesh, in_specs=in_specs, out_specs=out_specs, check_vma=False
    )
```

profile of v0, /device:TPU:0, one launch (start us, length us, event | category | flops | bytes accessed | tf_op | source)
XLA Modules:
  0.0 142.8 jit_solution(7347849369116743144)
XLA Ops:
  6.5 0.0 copy-start
  6.5 0.0 copy-start.2
  6.5 0.9 compare_reduce_fusion
  7.5 0.2 reduce_window_sum.11
  7.7 1.1 fusion.7
  8.8 1.6 %convolution_convert_fusion = bf16[4,64,2048]{2,1,0:T(8,128)(2,1)S(1)} fusion(s32[4,64]{1,0:T(4,128)S(1)} %broadcast_add_fusion, pred[4,64]{1,0:T(4,128)(4,1)S(1)} %bitcast.31, bf16[64,2048]{1,0:T(8,128)(2,1)} %param.10, f32[2048]{0:T(1024)} %param.11, f32[64]{0:T(128)S(1)} %add_rsqrt_fusion), kind=kOutput, calls=%fused_computation | convolution fusion | flops 68190208 | bytes 1320448 | tf_op jit(solution)/shard_map/kct,td->kcd/dot_general | solution.py:61
  10.4 0.0 copy-start.6
  10.4 32.0 %all_to_all.10 = bf16[4,64,2048]{2,1,0:T(8,128)(2,1)S(1)} all-to-all(bf16[4,64,2048]{2,1,0:T(8,128)(2,1)S(1)} %convolution_convert_fusion), channel_id=1, replica_groups=mesh['grp'=1,'ep'=4,'tp'=8] {'ep'}, dimensions={0} | all-to-all | bytes 2097152 | tf_op jit(solution)/shard_map/all_to_all | solution.py:64
  42.4 0.0 copy-done.2
  42.4 0.4 fusion.5
  42.9 0.0 copy-done.6
  42.9 0.4 fusion
  43.3 0.0 copy-done
  43.3 1.8 %fusion.2 = f32[4,64,2048]{2,1,0:T(8,128)} fusion(bf16[4,64,256]{2,1,0:T(8,128)(2,1)S(1)} %bitcast.29, bf16[1,256,2048]{2,1,0:T(8,128)(2,1)S(1)} %copy-done), kind=kOutput, calls=%fused_computation.7 | convolution fusion | flops 268435456 | bytes 3276800 | tf_op jit(solution)/shard_map/dot_general | solution.py:23
  45.1 0.0 copy-start.4
  45.1 0.0 copy-start.5
  45.1 0.0 copy-start.1
  45.1 0.0 copy-start.3
  45.1 3.8 %all-to-all-start.1 = ((f32[4,64,2048]{2,1,0:T(8,128)}), f32[4,64,2048]{2,1,0:T(8,128)S(1)}, u32[]{:S(2)}, u32[]{:S(2)}) async-start(f32[4,64,2048]{2,1,0:T(8,128)} %fusion.2), calls=%async_computation.1 | async-start | bytes 4194304 | tf_op jit(solution)/shard_map/all_to_all | solution.py:70
  48.9 0.0 reduce-scatter.2.cloned.1.call-start
  48.9 0.0 copy-done.4
  49.0 0.0 copy-done.5
  49.0 0.1 fusion.26
  49.1 0.0 copy-done.1
  49.1 0.0 copy-done.3
  49.1 1.2 fusion.32
  50.3 45.9 %all-to-all-done.1 = f32[4,64,2048]{2,1,0:T(8,128)S(1)} async-done(((f32[4,64,2048]{2,1,0:T(8,128)}), f32[4,64,2048]{2,1,0:T(8,128)S(1)}, u32[]{:S(2)}, u32[]{:S(2)}) %all-to-all-start.1) | async-done | bytes 2097184 | tf_op jit(solution)/shard_map/all_to_all | solution.py:70
  96.3 2.3 %convolution_bitcast_fusion = f32[64,2048]{1,0:T(8,128)} fusion(f32[4,64,2048]{2,1,0:T(8,128)S(1)} %all-to-all-done.1, f32[4,64]{1,0:T(4,128)S(1)} %bitcast.30, s32[4,64]{1,0:T(4,128)S(1)} %broadcast_add_fusion, pred[4,64]{1,0:T(4,128)(4,1)S(1)} %bitcast.32), kind=kOutput, calls=%fused_computation.2 | convolution fusion | flops 402702336 | bytes 2623744 | tf_op jit(solution)/shard_map/kct,kcd->td/dot_general | solution.py:72
  98.6 2.6 %convolution_add_fusion = f32[64,2048]{1,0:T(8,128)} fusion(f32[64,2048]{1,0:T(8,128)} %convolution_bitcast_fusion, bf16[64,2048]{1,0:T(8,128)(2,1)} %param.19, bf16[2048,64]{0,1:T(8,128)(2,1)} %param.18, f32[64,64]{1,0:T(8,128)S(1)} %fusion.32, bf16[64,2048]{1,0:T(8,128)(2,1)S(1)} %copy-done.1, f32[2048]{0:T(1024)S(1)} %copy-done.3, f32[64]{0:T(128)S(1)} %add_rsqrt_fusion), kind=kOutput, calls=%fused_computation.1 | convolution fusion | flops 34234368 | bytes 1859840 | tf_op jit(solution)/shard_map/dot_general | solution.py:23
  101.1 0.0 reduce-scatter.2.cloned.1.call-update
  101.1 33.4 %reduce-scatter.2.cloned.1.call-done = f32[64,256]{1,0:T(8,128)} async-done(((f32[64,2048]{1,0:T(8,128)}), f32[64,256]{1,0:T(8,128)}) %reduce-scatter.2.cloned.1.call-update) | async-done | bytes 65552 | tf_op jit(solution)/shard_map/reduce_scatter | solution.py:74
  134.5 1.5 %convert_element_type.29 = bf16[64,256]{1,0:T(8,128)(2,1)} convert(f32[64,256]{1,0:T(8,128)} %reduce-scatter.2.cloned.1.call-done) | non-fusion elementwise | flops 16384 | bytes 98304 | tf_op jit(solution)/shard_map/convert_element_type | solution.py:74
  (6 shorter events, 0.1 us)
Async XLA Ops:
  6.5 36.8 %copy-start = (bf16[1,256,2048]{2,1,0:T(8,128)(2,1)S(1)}, bf16[1,256,2048]{2,1,0:T(8,128)(2,1)}, u32[]{:S(2)}) copy-start(bf16[1,256,2048]{2,1,0:T(8,128)(2,1)} %param.16) | copy-start | bytes 3145732
  6.5 35.9 %copy-start.2 = (bf16[1,2048,256]{2,1,0:T(8,128)(2,1)S(1)}, bf16[1,2048,256]{2,1,0:T(8,128)(2,1)}, u32[]{:S(2)}) copy-start(bf16[1,2048,256]{2,1,0:T(8,128)(2,1)} %param.14) | copy-start | bytes 3145732
  10.4 32.5 %copy-start.6 = (bf16[1,2048,256]{2,1,0:T(8,128)(2,1)S(1)}, bf16[1,2048,256]{2,1,0:T(8,128)(2,1)}, u32[]{:S(2)}) copy-start(bf16[1,2048,256]{2,1,0:T(8,128)(2,1)} %param.15) | copy-start | bytes 3145732
  45.1 3.8 %copy-start.4 = (f32[64,8]{0,1:T(8,128)S(1)}, f32[64,8]{0,1:T(8,128)}, u32[]{:S(2)}) copy-start(f32[64,8]{0,1:T(8,128)} %param.13) | copy-start | bytes 6148
  45.1 3.9 %copy-start.5 = (s32[64,8]{0,1:T(8,128)S(1)}, s32[64,8]{0,1:T(8,128)}, u32[]{:S(2)}) copy-start(s32[64,8]{0,1:T(8,128)} %param.12) | copy-start | bytes 6148
  45.1 4.0 %copy-start.1 = (bf16[64,2048]{1,0:T(8,128)(2,1)S(1)}, bf16[64,2048]{1,0:T(8,128)(2,1)}, u32[]{:S(2)}) copy-start(bf16[64,2048]{1,0:T(8,128)(2,1)} %param.10) | copy-start | bytes 786436
  45.1 4.0 %copy-start.3 = (f32[2048]{0:T(1024)S(1)}, f32[2048]{0:T(1024)}, u32[]{:S(2)}) copy-start(f32[2048]{0:T(1024)} %param.11) | copy-start | bytes 24580
  45.1 51.1 %all-to-all-start.1 = ((f32[4,64,2048]{2,1,0:T(8,128)}), f32[4,64,2048]{2,1,0:T(8,128)S(1)}, u32[]{:S(2)}, u32[]{:S(2)}) async-start(f32[4,64,2048]{2,1,0:T(8,128)} %fusion.2), calls=%async_computation.1 | async-start | bytes 4194304 | tf_op jit(solution)/shard_map/all_to_all | solution.py:70
  48.9 85.6 %reduce-scatter.2.cloned.1.call-start = ((), (), s32[]{:S(2)}) async-start(), calls=%async_computation.3 | async-start | bytes 589824 | tf_op jit(solution)/shard_map/reduce_scatter | solution.py:74
Sparse Core Ops, SparseCore 0:
  101.3 33.1 reduce-scatter.1
where the time goes:
time: 143 us
  waiting for transfers between devices  79.3 us (55%)
  blocking collectives  32 us (22%)
  between operations  13.5 us (9%)
  matrix products  10.3 us (7%)
  other arithmetic  3.86 us (3%)
  starting transfers between devices  3.79 us (3%)
    all_to_all x1, waiting for transfers between devices, per_device(): lax.all_to_all(produced, 'ep', split_axis=0, concat_axis=0, tiled=True)  45.9 us
    reduce_scatter x1, waiting for transfers between devices, per_device(): lax.psum_scatter(routed + shared_term, 'tp', scatter_dimension=1, tiled=T...  33.4 us
    all_to_all x1, blocking collectives, per_device(): lax.all_to_all(outgoing, 'ep', split_axis=0, concat_axis=0, tiled=True)  32 us
    dot_general x2, matrix products, expert_apply(): return jnp.dot(active, down_half, preferred_element_type=jnp.float32)  4.35 us
    all_to_all x1, starting transfers between devices, per_device(): lax.all_to_all(produced, 'ep', split_axis=0, concat_axis=0, tiled=True)  3.75 us
  transfers between devices with their start and end apart: 2, of which 2 were waited for; matrix products, arithmetic and copies ran while one was open for 1% of the time, Pallas kernels for 0%

commit v1 on v0

v1 whole, which is shorter than its diff:
```python
import functools

import jax
import jax.numpy as jnp
from jax import lax
from jax.experimental import pallas as pl
from jax.experimental.pallas import tpu as pltpu
from jax.sharding import PartitionSpec as P

EXPERT_SHARDS = 2
CORES = 2
MESH = pl.DeviceIdType.MESH

eps = 1e-06
routed_scale = 2.5


def norm_rows(tokens, norm_gain):
    values = tokens.astype(jnp.float32)
    scaled = values * lax.rsqrt(jnp.mean(values * values, axis=-1, keepdims=True) + eps)
    return (scaled * norm_gain).astype(jnp.bfloat16)


def silu(value):
    return value / (1.0 + jnp.exp(-value))


def kernel(
    n_ep,
    n_tp,
    tok_hbm,
    gain_hbm,
    routes_hbm,
    score_hbm,
    gate_hbm,
    up_hbm,
    down_hbm,
    sgate_hbm,
    sup_hbm,
    sdown_hbm,
    out_ref,
    tok,
    gain,
    routes,
    score,
    gate,
    up,
    down,
    sgate,
    sup,
    sdown,
    gathered,
    part,
    part_in,
    pair,
    pair_in,
    plane,
    plane_in,
    kept,
    load_sem,
    z_send,
    z_recv,
    xy_send,
    xy_recv,
    d2d_send,
    d2d_recv,
    a_send,
    a_recv,
    b_send,
    b_recv,
    c_send,
    c_recv,
):
    chips = n_tp // CORES
    me = lax.axis_index("ep")
    seat = lax.axis_index("tp")
    chip, core = seat // CORES, seat % CORES
    rows, width = tok.shape
    half = rows // CORES
    chip_cols = width // chips
    out_cols = width // n_tp
    groups = group_count(n_ep)
    span = (n_ep - 1) // groups
    expert = me * (n_tp // EXPERT_SHARDS) + chip

    partner = {"tp": chip * CORES + 1 - core}
    plane_chip = [lax.rem(chip + j, chips) for j in range(chips)]
    plane_peer = [{"tp": c * CORES + core} for c in plane_chip]
    forward = [{"ep": lax.rem(me + d, n_ep)} for d in range(n_ep)]
    backward = [{"ep": lax.rem(me + n_ep - d, n_ep)} for d in range(n_ep)]

    def remote(src, dst, send, recv, target):
        return pltpu.make_async_remote_copy(
            src_ref=src, dst_ref=dst, send_sem=send, recv_sem=recv, device_id=target, device_id_type=MESH
        )

    loads = [
        pltpu.make_async_copy(src, dst, load_sem.at[i])
        for i, (src, dst) in enumerate(
            [
                (tok_hbm, tok),
                (routes_hbm, routes.at[0]),
                (score_hbm, score.at[0]),
                (gain_hbm, gain),
                (gate_hbm.at[0], gate),
                (up_hbm.at[0], up),
                (sgate_hbm, sgate),
                (sup_hbm, sup),
                (down_hbm.at[0], down),
                (sdown_hbm, sdown),
            ]
        )
    ]
    for load in loads:
        load.start()

    barrier = pltpu.get_barrier_semaphore()
    targets = forward[1:] + plane_peer[1:] + [partner]
    for target in targets:
        pl.semaphore_signal(barrier, inc=1, device_id=target, device_id_type=MESH)
    for load in loads[:3]:
        load.wait()
    pl.semaphore_wait(barrier, len(targets))

    my_rows = pl.ds(pl.multiple_of(core * half, half), half)
    my_cols = pl.ds(pl.multiple_of(chip * chip_cols, chip_cols), chip_cols)

    z_copies = []
    for d in range(1, n_ep):
        z_copies.append(
            [
                remote(
                    tok.at[my_rows, my_cols],
                    gathered.at[d - 1, my_rows, my_cols],
                    z_send.at[0, d - 1],
                    z_recv.at[0, d - 1],
                    forward[d],
                ),
                remote(routes.at[0], routes.at[d], z_send.at[1, d - 1], z_recv.at[1, d - 1], forward[d]),
                remote(score.at[0], score.at[d], z_send.at[2, d - 1], z_recv.at[2, d - 1], forward[d]),
            ]
        )
    for copies in z_copies:
        for copy in copies:
            copy.start()

    diagonal = lax.broadcasted_iota(jnp.int32, (rows, rows), 0) == lax.broadcasted_iota(
        jnp.int32, (rows, rows), 1
    )

    def row_weight(slot):
        scores = score[slot]
        mixing = scores / jnp.sum(scores, axis=0, keepdims=True) * routed_scale
        lane = jnp.sum(jnp.where(routes[slot] == expert, mixing, 0.0), axis=0, keepdims=True)
        return jnp.sum(jnp.where(diagonal, lane, 0.0), axis=1, keepdims=True)

    def span_of(group):
        if group == 0:
            return 0, 1
        return 1 + (group - 1) * span, span

    a_copies, b_copies = [], []

    def compute(group):
        first, count = span_of(group)
        raw = tok[...] if group == 0 else gathered[first - 1 : first - 1 + count].reshape(count * rows, width)
        normed = norm_rows(raw, gain[...])
        if group == 0:
            for load in loads[4:8]:
                load.wait()
        gate_part = jnp.dot(normed, gate[...], preferred_element_type=jnp.float32)
        upper = jnp.dot(normed, up[...], preferred_element_type=jnp.float32)
        weight = [row_weight(slot) for slot in range(first, first + count)]
        weight = weight[0] if count == 1 else jnp.concatenate(weight, axis=0)
        active = (silu(gate_part) * upper * weight).astype(jnp.bfloat16)
        if group == 0:
            contract = (((1,), (1,)), ((), ()))
            shared_gate = lax.dot_general(normed, sgate[...], contract, preferred_element_type=jnp.float32)
            shared_up = lax.dot_general(normed, sup[...], contract, preferred_element_type=jnp.float32)
            shared = (silu(shared_gate) * shared_up).astype(jnp.bfloat16)
            for load in loads[8:]:
                load.wait()
        for c in range(chips):
            cols = slice(c * chip_cols, (c + 1) * chip_cols)
            value = jnp.dot(active, down[:, cols], preferred_element_type=jnp.float32)
            if group == 0:
                value = value + jnp.dot(shared, sdown[:, cols], preferred_element_type=jnp.float32)
            value = value.astype(jnp.bfloat16)
            for s in range(count):
                for k in range(CORES):
                    part[first + s, k, c] = value[
                        s * rows : (s + 1) * rows, k * out_cols : (k + 1) * out_cols
                    ]
        copy = remote(
            part.at[pl.ds(first, count), 1 - core],
            part_in.at[pl.ds(first, count)],
            a_send.at[group],
            a_recv.at[group],
            partner,
        )
        copy.start()
        a_copies.append(copy)

    def pair_sum(slots, c):
        return part[slots, core, c].astype(jnp.float32) + part_in[slots, c].astype(jnp.float32)

    def reduce_pair(group):
        first, count = span_of(group)
        slots = pl.ds(first, count)
        a_copies[group].wait_recv()
        copies = []
        for j in range(1, chips):
            c = plane_chip[j]
            pair[slots, c] = pair_sum(slots, c).astype(jnp.bfloat16)
            copy = remote(
                pair.at[slots, c],
                pair_in.at[slots, j - 1],
                b_send.at[group, j - 1],
                b_recv.at[group, j - 1],
                plane_peer[j],
            )
            copy.start()
            copies.append(copy)
        b_copies.append(copies)

    c_copies = []

    def reduce_plane(group):
        first, count = span_of(group)
        slots = pl.ds(first, count)
        total = pair_sum(slots, chip)
        for j in range(1, chips):
            b_copies[group][j - 1].wait_recv()
            total = total + pair_in[slots, j - 1].astype(jnp.float32)
        if group == 0:
            kept[...] = total[0]
            return
        plane[pl.ds(first - 1, count)] = total.astype(jnp.bfloat16)
        for d in range(first, first + count):
            copy = remote(
                plane.at[d - 1], plane_in.at[d - 1], c_send.at[d - 1], c_recv.at[d - 1], backward[d]
            )
            copy.start()
            c_copies.append(copy)

    xy_copies = []

    def spread(group):
        first, count = span_of(group)
        for d in range(first, first + count):
            z_copies[d - 1][0].wait_recv()
        block = gathered.at[pl.ds(first - 1, count), my_rows, my_cols]
        copies = []
        for j in range(1, chips):
            copy = remote(
                block, block, xy_send.at[group - 1, j - 1], xy_recv.at[group - 1, j - 1], plane_peer[j]
            )
            copy.start()
            copies.append(copy)
        xy_copies.append(copies)

    d2d_copies = []

    def swap(group):
        first, count = span_of(group)
        for copy in xy_copies[group - 1]:
            copy.wait_recv()
        block = gathered.at[pl.ds(first - 1, count), my_rows]
        copy = remote(block, block, d2d_send.at[group - 1], d2d_recv.at[group - 1], partner)
        copy.start()
        d2d_copies.append(copy)

    def arrive(group):
        first, count = span_of(group)
        for d in range(first, first + count):
            z_copies[d - 1][1].wait_recv()
            z_copies[d - 1][2].wait_recv()
        d2d_copies[group - 1].wait_recv()

    loads[3].wait()
    compute(0)
    for group in range(1, groups + 1):
        spread(group)
    reduce_pair(0)
    swap(1)
    for group in range(1, groups + 1):
        if group < groups:
            swap(group + 1)
        if group > 1:
            reduce_pair(group - 1)
        arrive(group)
        compute(group)
        if group > 1:
            reduce_plane(group - 1)
    reduce_pair(groups)
    reduce_plane(0)
    reduce_plane(groups)
    total = kept[...]
    for d in range(1, n_ep):
        c_copies[d - 1].wait_recv()
        total = total + plane_in[d - 1].astype(jnp.float32)
    out_ref[...] = total.astype(jnp.bfloat16)
    everything = sum(z_copies + xy_copies + b_copies, []) + d2d_copies + a_copies + c_copies
    for copy in everything:
        copy.wait_send()


def group_count(n_ep):
    return 3 if (n_ep - 1) % 3 == 0 else n_ep - 1


def per_device(
    tokens,
    norm_gain,
    routes,
    route_weight,
    gate_proj,
    up_proj,
    down_proj,
    shared_gate,
    shared_up,
    shared_down,
):
    n_ep = lax.axis_size("ep")
    n_tp = lax.axis_size("tp")
    chips = n_tp // CORES
    rows, width = tokens.shape
    out_cols = width // n_tp
    top_count = routes.shape[1]
    hidden = gate_proj.shape[2]
    shared = shared_gate.shape[1]
    groups = group_count(n_ep)
    bf16, f32 = jnp.bfloat16, jnp.float32
    dma = pltpu.SemaphoreType.DMA
    operands = (
        tokens,
        norm_gain.reshape(1, width),
        routes.T,
        route_weight.T,
        gate_proj,
        up_proj,
        down_proj,
        shared_gate.T,
        shared_up.T,
        shared_down,
    )
    return pl.pallas_call(
        functools.partial(kernel, n_ep, n_tp),
        out_shape=jax.ShapeDtypeStruct((rows, out_cols), bf16),
        in_specs=[pl.BlockSpec(memory_space=pl.ANY)] * len(operands),
        out_specs=pl.BlockSpec(memory_space=pltpu.VMEM),
        scratch_shapes=[
            pltpu.VMEM((rows, width), bf16),
            pltpu.VMEM((1, width), f32),
            pltpu.VMEM((n_ep, top_count, rows), jnp.int32),
            pltpu.VMEM((n_ep, top_count, rows), f32),
            pltpu.VMEM((width, hidden), bf16),
            pltpu.VMEM((width, hidden), bf16),
            pltpu.VMEM((hidden, width), bf16),
            pltpu.VMEM((shared, width), bf16),
            pltpu.VMEM((shared, width), bf16),
            pltpu.VMEM((shared, width), bf16),
            pltpu.VMEM((n_ep - 1, rows, width), bf16),
            pltpu.VMEM((n_ep, CORES, chips, rows, out_cols), bf16),
            pltpu.VMEM((n_ep, chips, rows, out_cols), bf16),
            pltpu.VMEM((n_ep, chips, rows, out_cols), bf16),
            pltpu.VMEM((n_ep, chips - 1, rows, out_cols), bf16),
            pltpu.VMEM((n_ep - 1, rows, out_cols), bf16),
            pltpu.VMEM((n_ep - 1, rows, out_cols), bf16),
            pltpu.VMEM((rows, out_cols), f32),
            dma((len(operands),)),
            dma((3, n_ep - 1)),
            dma((3, n_ep - 1)),
            dma((groups, chips - 1)),
            dma((groups, chips - 1)),
            dma((groups,)),
            dma((groups,)),
            dma((groups + 1,)),
            dma((groups + 1,)),
            dma((groups + 1, chips - 1)),
            dma((groups + 1, chips - 1)),
            dma((n_ep - 1,)),
            dma((n_ep - 1,)),
        ],
        compiler_params=pltpu.CompilerParams(
            collective_id=0, has_side_effects=True, vmem_limit_bytes=60 * 1024 * 1024
        ),
    )(*operands)


def solution(mesh):
    in_specs = (
        P(("grp", "ep"), None),
        P(),
        P(("grp", "ep"), None),
        P(("grp", "ep"), None),
        P(("ep", "tp"), None, None),
        P(("ep", "tp"), None, None),
        P(("ep", "tp"), None, None),
        P(None, "tp"),
        P(None, "tp"),
        P("tp", None),
    )
    out_specs = P(("grp", "ep"), "tp")
    return jax.shard_map(
        per_device, mesh=mesh, in_specs=in_specs, out_specs=out_specs, check_vma=False
    )
```

time: 143 us -> 33.2 us (0.23)
  waiting for transfers between devices: 79.3 us -> 0 us
  blocking collectives: 32 us -> 0 us
  Pallas kernels: 0 us -> 31.7 us
  between operations: 13.5 us -> 0.01 us
  matrix products: 10.3 us -> 0 us
  other arithmetic: 3.86 us -> 0 us
  starting transfers between devices: 3.79 us -> 0 us
    all_to_all x1 -> x0, waiting for transfers between devices: 45.9 us -> none  [per_device(): lax.all_to_all(produced, 'ep', split_axis=0, concat_axis=0, tiled=True)]
    reduce_scatter x1 -> x0, waiting for transfers between devices: 33.4 us -> none  [per_device(): lax.psum_scatter(routed + shared_term, 'tp', scatter_dimension=1, tiled=T...]
    all_to_all x1 -> x0, blocking collectives: 32 us -> none  [per_device(): lax.all_to_all(outgoing, 'ep', split_axis=0, concat_axis=0, tiled=True)]
    pallas_call x0 -> x1, Pallas kernels: none -> 31.7 us  [per_device(): pl.pallas_call(functools.partial(kernel, n_ep, n_tp), out_shape=jax.Shape...]
    dot_general x7 -> x0, matrix products: 10.3 us -> none  [the longest x2 4.35 us: expert_apply(): return jnp.dot(active, down_half, preferred_element_type=jnp.float32)]
    all_to_all x1 -> x0, starting transfers between devices: 3.75 us -> none  [per_device(): lax.all_to_all(produced, 'ep', split_axis=0, concat_axis=0, tiled=True)]
    convert_element_type x2 -> x0, other arithmetic: 1.46 us -> none  [the longest x1 1.46 us: per_device(): lax.psum_scatter(routed + shared_term, 'tp', scatter_dimension=1, tiled=T...]
  transfers between devices with their start and end apart: 2 -> 0, of which waited for: 2 -> 0; matrix products, arithmetic and copies ran while one was open for 1% -> 0% of each run, Pallas kernels for 0% -> 0%
where the time goes in v1:
time: 33.2 us; the launch traced here: 33.1 us
  Pallas kernels  31.7 us (95%)
  local copies, waits for them, and re-layouts  1.38 us (4%)
    pallas_call x1, Pallas kernels, per_device(): pl.pallas_call(functools.partial(kernel, n_ep, n_tp), out_shape=jax.Shape...  31.7 us
    unnamed x1, local copies, waits for them, and re-layouts  1.38 us

profile of v1, /device:TPU:0, one launch (start us, length us, event | category | flops | bytes accessed | tf_op | source)
XLA Modules:
  0.0 33.1 jit_solution(11766357662070357158)
XLA Ops:
  0.0 31.7 %shard_map.100 = bf16[64,256]{1,0:T(8,128)(2,1)} custom-call(bf16[64,2048]{1,0:T(8,128)(2,1)} %tok_hbm.1, f32[1,2048]{1,0:T(1,128)} %bitcast.7, s32[8,64]{1,0:T(8,128)} %bitcast.8, f32[8,64]{1,0:T(8,128)} %bitcast.9, bf16[1,2048,256]{2,1,0:T(8,128)(2,1)} %gate_hbm.1, bf16[1,2048,256]{2,1,0:T(8,128)(2,1)} %up_hbm.1, bf16[1,256,2048]{2,1,0:T(8,128)(2,1)} %down_hbm.1, ...), custom_call_target="tpu_custom_call" | custom-call | tf_op jit(solution)/shard_map/pallas_call | solution.py:347
  31.7 1.4 %copy.12 = bf16[64,256]{1,0:T(8,128)(2,1)} copy(bf16[64,256]{1,0:T(8,128)(2,1)} %shard_map.100) | data formatting | bytes 65536

commit v2 on v1

--- a/solution.py
+++ b/solution.py
@@ -84,10 +84,11 @@
     expert = me * (n_tp // EXPERT_SHARDS) + chip
 
     partner = {"tp": chip * CORES + 1 - core}
-    plane_chip = [lax.rem(chip + j, chips) for j in range(chips)]
+    plane_chip = [flipped(chip, j, chips) for j in range(chips)]
+    plane_order = list(range(chips - 1, 0, -1))
     plane_peer = [{"tp": c * CORES + core} for c in plane_chip]
-    forward = [{"ep": lax.rem(me + d, n_ep)} for d in range(n_ep)]
-    backward = [{"ep": lax.rem(me + n_ep - d, n_ep)} for d in range(n_ep)]
+    others = [lax.rem(me + d, n_ep) for d in range(n_ep)]
+    forward = [{"ep": other} for other in others]
 
     def remote(src, dst, send, recv, target):
         return pltpu.make_async_remote_copy(
@@ -125,24 +126,24 @@
     my_rows = pl.ds(pl.multiple_of(core * half, half), half)
     my_cols = pl.ds(pl.multiple_of(chip * chip_cols, chip_cols), chip_cols)
 
-    z_copies = []
-    for d in range(1, n_ep):
-        z_copies.append(
-            [
-                remote(
-                    tok.at[my_rows, my_cols],
-                    gathered.at[d - 1, my_rows, my_cols],
-                    z_send.at[0, d - 1],
-                    z_recv.at[0, d - 1],
-                    forward[d],
-                ),
-                remote(routes.at[0], routes.at[d], z_send.at[1, d - 1], z_recv.at[1, d - 1], forward[d]),
-                remote(score.at[0], score.at[d], z_send.at[2, d - 1], z_recv.at[2, d - 1], forward[d]),
-            ]
-        )
-    for copies in z_copies:
-        for copy in copies:
-            copy.start()
+    def z_pieces(source, slot, target):
+        return [
+            remote(
+                tok.at[my_rows, my_cols],
+                gathered.at[slot - 1, my_rows, my_cols],
+                z_send.at[0, source],
+                z_recv.at[0, slot - 1],
+                target,
+            ),
+            remote(routes.at[0], routes.at[slot], z_send.at[1, source], z_recv.at[1, slot - 1], target),
+            remote(score.at[0], score.at[slot], z_send.at[2, source], z_recv.at[2, slot - 1], target),
+        ]
+
+    z_copies = [z_pieces(d - 1, place_of(me, others[d], n_ep), forward[d]) for d in range(1, n_ep)]
+    z_arrivals = [z_pieces(slot - 1, slot, forward[1]) for slot in range(1, n_ep)]
+    for piece in range(3):
+        for copies in z_copies:
+            copies[piece].start()
 
     diagonal = lax.broadcasted_iota(jnp.int32, (rows, rows), 0) == lax.broadcasted_iota(
         jnp.int32, (rows, rows), 1
@@ -180,8 +181,10 @@
             shared = (silu(shared_gate) * shared_up).astype(jnp.bfloat16)
             for load in loads[8:]:
                 load.wait()
-        for c in range(chips):
-            cols = slice(c * chip_cols, (c + 1) * chip_cols)
+        copies = [None] * chips
+        for j in plane_order + [0]:
+            c = plane_chip[j]
+            cols = pl.ds(pl.multiple_of(c * chip_cols, chip_cols), chip_cols)
             value = jnp.dot(active, down[:, cols], preferred_element_type=jnp.float32)
             if group == 0:
                 value = value + jnp.dot(shared, sdown[:, cols], preferred_element_type=jnp.float32)
@@ -191,15 +194,15 @@
                     part[first + s, k, c] = value[
                         s * rows : (s + 1) * rows, k * out_cols : (k + 1) * out_cols
                     ]
-        copy = remote(
-            part.at[pl.ds(first, count), 1 - core],
-            part_in.at[pl.ds(first, count)],
-            a_send.at[group],
-            a_recv.at[group],
-            partner,
-        )
-        copy.start()
-        a_copies.append(copy)
+            copies[j] = remote(
+                part.at[pl.ds(first, count), 1 - core, c],
+                part_in.at[pl.ds(first, count), c],
+                a_send.at[group, j],
+                a_recv.at[group, j],
+                partner,
+            )
+            copies[j].start()
+        a_copies.append(copies)
 
     def pair_sum(slots, c):
         return part[slots, core, c].astype(jnp.float32) + part_in[slots, c].astype(jnp.float32)
@@ -207,20 +210,20 @@
     def reduce_pair(group):
         first, count = span_of(group)
         slots = pl.ds(first, count)
-        a_copies[group].wait_recv()
-        copies = []
-        for j in range(1, chips):
+        copies = [None] * chips
+        for j in plane_order:
             c = plane_chip[j]
+            a_copies[group][j].wait_recv()
             pair[slots, c] = pair_sum(slots, c).astype(jnp.bfloat16)
-            copy = remote(
+            copies[j] = remote(
                 pair.at[slots, c],
                 pair_in.at[slots, j - 1],
                 b_send.at[group, j - 1],
                 b_recv.at[group, j - 1],
                 plane_peer[j],
             )
-            copy.start()
-            copies.append(copy)
+            copies[j].start()
+        a_copies[group][0].wait_recv()
         b_copies.append(copies)
 
     c_copies = []
@@ -230,52 +233,61 @@
         slots = pl.ds(first, count)
         total = pair_sum(slots, chip)
         for j in range(1, chips):
-            b_copies[group][j - 1].wait_recv()
+            b_copies[group][j].wait_recv()
             total = total + pair_in[slots, j - 1].astype(jnp.float32)
         if group == 0:
             kept[...] = total[0]
             return
         plane[pl.ds(first - 1, count)] = total.astype(jnp.bfloat16)
         for d in range(first, first + count):
+            source = source_of(me, d, n_ep)
+            there = lax.rem(source - me + n_ep, n_ep) - 1
             copy = remote(
-                plane.at[d - 1], plane_in.at[d - 1], c_send.at[d - 1], c_recv.at[d - 1], backward[d]
+                plane.at[d - 1], plane_in.at[there], c_send.at[d - 1], c_recv.at[there], {"ep": source}
             )
             copy.start()
             c_copies.append(copy)
 
-    xy_copies = []
+    xy_copies, d2d_copies = [], []
+
+    def block_of(group, c):
+        first, count = span_of(group)
+        cols = pl.ds(pl.multiple_of(c * chip_cols, chip_cols), chip_cols)
+        return gathered.at[pl.ds(first - 1, count), my_rows, cols]
+
+    def swap_piece(group, j):
+        block = block_of(group, plane_chip[j])
+        copy = remote(block, block, d2d_send.at[group - 1, j], d2d_recv.at[group - 1, j], partner)
+        copy.start()
+        d2d_copies[group - 1].append(copy)
 
     def spread(group):
         first, count = span_of(group)
         for d in range(first, first + count):
-            z_copies[d - 1][0].wait_recv()
-        block = gathered.at[pl.ds(first - 1, count), my_rows, my_cols]
-        copies = []
-        for j in range(1, chips):
-            copy = remote(
+            z_arrivals[d - 1][0].wait_recv()
+        block = block_of(group, chip)
+        copies = [None] * chips
+        for j in plane_order:
+            copies[j] = remote(
                 block, block, xy_send.at[group - 1, j - 1], xy_recv.at[group - 1, j - 1], plane_peer[j]
             )
-            copy.start()
-            copies.append(copy)
+            copies[j].start()
         xy_copies.append(copies)
-
-    d2d_copies = []
+        d2d_copies.append([])
+        swap_piece(group, 0)
 
     def swap(group):
-        first, count = span_of(group)
-        for copy in xy_copies[group - 1]:
+        for j in plane_order[::-1]:
+            xy_copies[group - 1][j].wait_recv()
+            swap_piece(group, j)
+
+    def arrive(group):
+        first, count = span_of(group)
+        for d in range(first, first + count):
+            z_arrivals[d - 1][1].wait_recv()
+            z_arrivals[d - 1][2].wait_recv()
+        for copy in d2d_copies[group - 1]:
             copy.wait_recv()
-        block = gathered.at[pl.ds(first - 1, count), my_rows]
-        copy = remote(block, block, d2d_send.at[group - 1], d2d_recv.at[group - 1], partner)
-        copy.start()
-        d2d_copies.append(copy)
-
-    def arrive(group):
-        first, count = span_of(group)
-        for d in range(first, first + count):
-            z_copies[d - 1][1].wait_recv()
-            z_copies[d - 1][2].wait_recv()
-        d2d_copies[group - 1].wait_recv()
 
     loads[3].wait()
     compute(0)
@@ -290,19 +302,52 @@
             reduce_pair(group - 1)
         arrive(group)
         compute(group)
-        if group > 1:
-            reduce_plane(group - 1)
-    reduce_pair(groups)
     reduce_plane(0)
+    for group in range(1, groups):
+        if group == groups - 1:
+            reduce_pair(groups)
+        reduce_plane(group)
     reduce_plane(groups)
     total = kept[...]
     for d in range(1, n_ep):
-        c_copies[d - 1].wait_recv()
+        remote(
+            plane.at[0], plane_in.at[d - 1], c_send.at[d - 1], c_recv.at[d - 1], forward[1]
+        ).wait_recv()
         total = total + plane_in[d - 1].astype(jnp.float32)
     out_ref[...] = total.astype(jnp.bfloat16)
-    everything = sum(z_copies + xy_copies + b_copies, []) + d2d_copies + a_copies + c_copies
+    everything = sum(z_copies + xy_copies + b_copies + d2d_copies + a_copies, []) + c_copies
     for copy in everything:
-        copy.wait_send()
+        if copy is not None:
+            copy.wait_send()
+
+
+def flipped(chip, j, chips):
+    assert chips & (chips - 1) == 0
+    out, bit = chip, 1
+    while bit < chips:
+        if j & bit:
+            out = out + bit - 2 * bit * (chip // bit % 2)
+        bit *= 2
+    return out
+
+
+def room(index, count):
+    side = jnp.minimum(index, count - 1 - index)
+    toward = jnp.where(index < count - 1 - index, 1, -1)
+    return side, toward
+
+
+def source_of(index, place, count):
+    side, toward = room(index, count)
+    near = (place + 1) // 2 * (1 if place % 2 else -1)
+    return index + toward * jnp.where(place <= 2 * side, near, place - side)
+
+
+def place_of(source, index, count):
+    side, toward = room(index, count)
+    away = jnp.abs(source - index)
+    same = (source - index) * toward > 0
+    return jnp.where(away <= side, 2 * away - jnp.where(same, 1, 0), away + side)
 
 
 def group_count(n_ep):
@@ -346,7 +391,7 @@
     )
     return pl.pallas_call(
         functools.partial(kernel, n_ep, n_tp),
-        out_shape=jax.ShapeDtypeStruct((rows, out_cols), bf16),
+        out_shape=pltpu.VMEM((rows, out_cols), bf16),
         in_specs=[pl.BlockSpec(memory_space=pl.ANY)] * len(operands),
         out_specs=pl.BlockSpec(memory_space=pltpu.VMEM),
         scratch_shapes=[
@@ -373,10 +418,10 @@
             dma((3, n_ep - 1)),
             dma((groups, chips - 1)),
             dma((groups, chips - 1)),
-            dma((groups,)),
-            dma((groups,)),
-            dma((groups + 1,)),
-            dma((groups + 1,)),
+            dma((groups, chips)),
+            dma((groups, chips)),
+            dma((groups + 1, chips)),
+            dma((groups + 1, chips)),
             dma((groups + 1, chips - 1)),
             dma((groups + 1, chips - 1)),
             dma((n_ep - 1,)),

time: 33.2 us -> 29.8 us (0.90)
  Pallas kernels: 31.7 us -> 29 us
  local copies, waits for them, and re-layouts: 1.38 us -> 0.62 us
    pallas_call x1, Pallas kernels: 31.7 us -> 29 us  [per_device(): pl.pallas_call(functools.partial(kernel, n_ep, n_tp), out_shape=pltpu.VME...]
    unnamed x1, local copies, waits for them, and re-layouts: 1.38 us -> 0.62 us
where the time goes in v2:
time: 29.8 us; the launch traced here: 29.6 us
  Pallas kernels  29 us (97%)
  local copies, waits for them, and re-layouts  0.62 us (2%)
    pallas_call x1, Pallas kernels, per_device(): pl.pallas_call(functools.partial(kernel, n_ep, n_tp), out_shape=pltpu.VME...  29 us
    unnamed x1, local copies, waits for them, and re-layouts  0.62 us

profile of v2, /device:TPU:0, one launch (start us, length us, event | category | flops | bytes accessed | tf_op | source)
XLA Modules:
  0.0 29.6 jit_solution(2044168450449944330)
XLA Ops:
  0.0 29.0 %shard_map.100 = bf16[64,256]{1,0:T(8,128)(2,1)S(1)} custom-call(bf16[64,2048]{1,0:T(8,128)(2,1)} %tok_hbm.1, f32[1,2048]{1,0:T(1,128)} %bitcast.7, s32[8,64]{1,0:T(8,128)} %bitcast.8, f32[8,64]{1,0:T(8,128)} %bitcast.9, bf16[1,2048,256]{2,1,0:T(8,128)(2,1)} %gate_hbm.1, bf16[1,2048,256]{2,1,0:T(8,128)(2,1)} %up_hbm.1, bf16[1,256,2048]{2,1,0:T(8,128)(2,1)} %down_hbm.1, ...), custom_call_target="tpu_custom_call" | custom-call | tf_op jit(solution)/shard_map/pallas_call | solution.py:392
  29.0 0.6 %copy.12 = bf16[64,256]{1,0:T(8,128)(2,1)} copy(bf16[64,256]{1,0:T(8,128)(2,1)S(1)} %shard_map.100) | data formatting | bytes 65536

commit v3 on v2

--- a/solution.py
+++ b/solution.py
@@ -87,7 +87,7 @@
     plane_chip = [flipped(chip, j, chips) for j in range(chips)]
     plane_order = list(range(chips - 1, 0, -1))
     plane_peer = [{"tp": c * CORES + core} for c in plane_chip]
-    others = [lax.rem(me + d, n_ep) for d in range(n_ep)]
+    others = [me] + [source_of(me, d, n_ep) for d in range(n_ep - 1, 0, -1)]
     forward = [{"ep": other} for other in others]
 
     def remote(src, dst, send, recv, target):
@@ -302,12 +302,9 @@
             reduce_pair(group - 1)
         arrive(group)
         compute(group)
-    reduce_plane(0)
-    for group in range(1, groups):
-        if group == groups - 1:
-            reduce_pair(groups)
+    reduce_pair(groups)
+    for group in range(groups + 1):
         reduce_plane(group)
-    reduce_plane(groups)
     total = kept[...]
     for d in range(1, n_ep):
         remote(

time: 29.8 us -> 29.2 us (0.980)
  Pallas kernels: 29 us -> 28.4 us
    pallas_call x1, Pallas kernels: 29 us -> 28.4 us  [per_device(): pl.pallas_call(functools.partial(kernel, n_ep, n_tp), out_shape=pltpu.VME...]
where the time goes in v3:
time: 29.2 us; the launch traced here: 29.1 us
  Pallas kernels  28.4 us (97%)
  local copies, waits for them, and re-layouts  0.62 us (2%)
    pallas_call x1, Pallas kernels, per_device(): pl.pallas_call(functools.partial(kernel, n_ep, n_tp), out_shape=pltpu.VME...  28.4 us
    unnamed x1, local copies, waits for them, and re-layouts  0.62 us

profile of v3, /device:TPU:0, one launch (start us, length us, event | category | flops | bytes accessed | tf_op | source)
XLA Modules:
  0.0 29.1 jit_solution(7434593702468541361)
XLA Ops:
  0.0 28.4 %shard_map.100 = bf16[64,256]{1,0:T(8,128)(2,1)S(1)} custom-call(bf16[64,2048]{1,0:T(8,128)(2,1)} %tok_hbm.1, f32[1,2048]{1,0:T(1,128)} %bitcast.7, s32[8,64]{1,0:T(8,128)} %bitcast.8, f32[8,64]{1,0:T(8,128)} %bitcast.9, bf16[1,2048,256]{2,1,0:T(8,128)(2,1)} %gate_hbm.1, bf16[1,2048,256]{2,1,0:T(8,128)(2,1)} %up_hbm.1, bf16[1,256,2048]{2,1,0:T(8,128)(2,1)} %down_hbm.1, ...), custom_call_target="tpu_custom_call" | custom-call | tf_op jit(solution)/shard_map/pallas_call | solution.py:389
  28.5 0.6 %copy.12 = bf16[64,256]{1,0:T(8,128)(2,1)} copy(bf16[64,256]{1,0:T(8,128)(2,1)S(1)} %shard_map.100) | data formatting | bytes 65536
